TPU v7x, 32 devices: a whole 2x2x4 slice. The times are simulated.
32 devices in a mesh: sp: 8 (over z, y), tp: 4 (over x, core).
Axes of the slice: x: 2, y: 2, z: 4, core: 2. Of those that a mesh axis runs over, the one named last changes fastest.
Arguments:
- stream: bfloat16 [2048, 2048], P('sp', 'tp'), may hold values from -1200 to 1200, as said below
- mix_gain: bfloat16 [2048], P('tp'), may hold values from 0.099609375 to 1.8984375
- pool_weight: bfloat16 [4, 512, 512], P('tp'), may hold values from -0.25 to 0.25
- pool_scale: bfloat16 [2048], P('tp'), may hold values from 0.099609375 to 1.8984375
- ffn_gain: bfloat16 [2048], replicated, may hold values from 0.099609375 to 1.8984375
- routes: int32 [2048, 2], P(('sp', 'tp')), may hold values from 0 to 7, all different within a row; in each aligned block of 64 rows (0 to 63, 64 to 127, ...) at most 32 rows name the same one
- route_weight: float32 [2048, 2], P(('sp', 'tp')), may hold values from 0.1 to 1
- w_gate: bfloat16 [8, 2048, 7168], P('sp', None, 'tp'), may hold values from -0.125 to 0.125
- w_up: bfloat16 [8, 2048, 7168], P('sp', None, 'tp'), may hold values from -0.125 to 0.125
- w_down: bfloat16 [8, 7168, 2048], P('sp', 'tp'), may hold values from -0.0625 to 0.0625
Outputs:
- layer_out: bfloat16 [2048, 2048], P(('sp', 'tp'))
Inputs may be any that keep to these rules, and one draw needn't show every extreme that they name: `routes`: each row names 2 different experts. Within each aligned block of 64 rows (the rows of one device) no expert is named by more than 32 rows, a bound that some block reaches. `stream`: finite values.
All inputs are finite; a program needn't handle non-finite values.
Results may differ from a plain program's by a relative error of at most 0.0061.
Values may be sent and summed in bfloat16 or wider, within the bound.
A program may use at most 128 MiB of HBM per device.

v0:
```python
import jax
import jax.numpy as jnp
from jax import lax
from jax.sharding import PartitionSpec as P

NORM_EPS = 1e-06


def passed_along(block, axis, distance):
    devices = range(lax.axis_size(axis))
    route = [(i - distance, i) for i in devices if i - distance in devices]
    return lax.ppermute(block, axis, route)


def expert_rows(arrived, w_gate, w_up, w_down):
    sp_count, tp_count, slot_count, model_width = arrived.shape
    flat_rows = arrived.reshape(-1, model_width)
    gate_val = jnp.dot(flat_rows, w_gate[0], preferred_element_type=jnp.float32)
    up_val = jnp.dot(flat_rows, w_up[0], preferred_element_type=jnp.float32)
    hidden = (jax.nn.silu(gate_val) * up_val).astype(jnp.bfloat16)
    block_out = jnp.dot(hidden, w_down[0], preferred_element_type=jnp.float32)
    block_out = block_out.reshape(sp_count, tp_count, slot_count, model_width)
    summed = lax.psum_scatter(block_out.astype(jnp.bfloat16), "tp", scatter_dimension=1, tiled=True)
    return summed.reshape(sp_count, slot_count, model_width)


def per_device(
    stream, mix_gain, pool_weight, pool_scale, ffn_gain, routes, route_weight, w_gate, w_up, w_down
):
    tok_rows, shard_width = stream.shape
    tp_count = lax.axis_size("tp")
    sp_count = lax.axis_size("sp")
    model_width = shard_width * tp_count
    stream_f32 = stream.astype(jnp.float32)
    square = lax.psum(jnp.sum(stream_f32 * stream_f32, axis=1), "tp")
    row_scale = lax.rsqrt(square / model_width + NORM_EPS)[:, None]
    normed = (stream_f32 * row_scale * mix_gain.astype(jnp.float32)).astype(jnp.bfloat16)
    local_groups = pool_weight.shape[0]
    halo_rows = 2 ** (local_groups * tp_count) - 1
    previous = passed_along(normed[tok_rows - halo_rows :], "sp", 1)
    extended = jnp.concatenate([previous, normed], axis=0)
    first_row = lax.axis_index("sp") * tok_rows
    position = first_row + jnp.arange(tok_rows, dtype=jnp.int32)
    source = first_row - halo_rows + jnp.arange(tok_rows + halo_rows, dtype=jnp.int32)
    lag_rows = position[:, None] - source[None, :]
    group_index = lax.axis_index("tp") * local_groups + 0
    window_len = jnp.left_shift(jnp.int32(2), group_index)
    band_mask = ((lag_rows >= 0) & (lag_rows < window_len)).astype(jnp.bfloat16)
    window_sum = jnp.dot(band_mask, extended, preferred_element_type=jnp.float32)
    window_count = jnp.minimum(position + 1, window_len).astype(jnp.float32)[:, None]
    own_rows = normed.astype(jnp.float32)
    pooled = (window_sum / window_count - own_rows).astype(jnp.bfloat16)
    group_outs = jnp.dot(pooled, pool_weight[0], preferred_element_type=jnp.float32)
    mixer_out = group_outs * pool_scale.astype(jnp.float32)
    after_mix = (stream_f32 + mixer_out).astype(jnp.bfloat16)
    token_rows = lax.all_to_all(after_mix, "tp", split_axis=0, concat_axis=1, tiled=True)
    after_f32 = token_rows.astype(jnp.float32)
    ffn_scale = lax.rsqrt(jnp.mean(after_f32 * after_f32, axis=1, keepdims=True) + NORM_EPS)
    normed2 = (after_f32 * ffn_scale * ffn_gain.astype(jnp.float32)).astype(jnp.bfloat16)
    tok_count, top_count = routes.shape
    capacity = 2 * tok_count * top_count // sp_count
    flat_routes = routes.reshape(-1)
    is_expert = (flat_routes[:, None] == jnp.arange(sp_count, dtype=jnp.int32)[None, :]).astype(
        jnp.int32
    )
    slot_rank = jnp.cumsum(is_expert, axis=0) - is_expert
    slot_index = jnp.sum(slot_rank * is_expert, axis=1)
    dest_slot = (flat_routes * capacity + slot_index).reshape(tok_count, top_count)
    slot_ids = jnp.arange(sp_count * capacity, dtype=jnp.int32)
    pick_masks = [
        (dest_slot[:, pick_index][None, :] == slot_ids[:, None]).astype(jnp.bfloat16)
        for pick_index in range(top_count)
    ]
    dispatch_mask = pick_masks[0]
    pick_index = 1
    dispatch_mask = dispatch_mask + pick_masks[pick_index]
    send_rows = jnp.dot(dispatch_mask, normed2, preferred_element_type=jnp.float32).astype(
        jnp.bfloat16
    )
    send_rows = send_rows.reshape(sp_count, capacity, model_width)
    shared = lax.all_gather(
        lax.all_to_all(send_rows, "sp", split_axis=0, concat_axis=0, tiled=True)[:, None],
        "tp",
        axis=1,
        tiled=True,
    )
    served = expert_rows(shared, w_gate, w_up, w_down)
    returned = lax.all_to_all(served, "sp", split_axis=0, concat_axis=0, tiled=True).reshape(
        sp_count * capacity, model_width
    )
    expert_sum = after_f32
    for pick_index in range(top_count):
        picked_out = jnp.dot(pick_masks[pick_index].T, returned, preferred_element_type=jnp.float32)
        expert_sum = expert_sum + route_weight[:, pick_index : pick_index + 1] * picked_out
    return expert_sum.astype(jnp.bfloat16)


def solution(mesh):
    in_specs = (
        P("sp", "tp"),
        P("tp"),
        P("tp", None, None),
        P("tp"),
        P(),
        P(("sp", "tp"), None),
        P(("sp", "tp"), None),
        P("sp", None, "tp"),
        P("sp", None, "tp"),
        P("sp", "tp", None),
    )
    out_specs = P(("sp", "tp"), None)
    return jax.shard_map(
        per_device, mesh=mesh, in_specs=in_specs, out_specs=out_specs, check_vma=False
    )
```

profile of v0, /device:TPU:0, one launch (start us, length us, event | category | flops | bytes accessed | tf_op | source)
XLA Modules:
  0.0 261.1 jit_solution(6128757934799268222)
XLA Ops:
  6.5 0.0 copy-start
  6.5 1.1 fusion.19
  7.7 8.4 %psum.7 = f32[256]{0:T(256)S(1)} all-reduce(f32[256]{0:T(256)S(1)} %fusion.19), channel_id=1, replica_groups=mesh['sp'=8,'tp'=4] {'tp'}, use_global_device_ids=true, to_apply=%region_1.0 | all-reduce | flops 256 | bytes 2048 | tf_op jit(solution)/shard_map/psum | solution.py:35
  16.1 0.7 convert_element_type.70
  16.7 1.1 fusion.21
  17.8 3.4 %collective-permute-start = (bf16[15,512]{1,0:T(8,128)(2,1)S(1)}, bf16[15,512]{1,0:T(8,128)(2,1)S(1)}, u32[]{:S(2)}, u32[]{:S(2)}) collective-permute-start(bf16[15,512]{1,0:T(8,128)(2,1)S(1)} %slice.20), channel_id=1, source_target_pairs={{0,4},{4,8},{8,12},{12,16},{16,20},{20,24},{24,28},{1,5},{5,9},{9,... | collective-permute-start | bytes 46088 | tf_op jit(solution)/shard_map/ppermute | solution.py:12
  21.3 0.8 copy.24
  22.1 0.1 eq.45
  22.2 0.1 fusion.53
  22.3 0.2 reduce_window_sum.11
  22.5 0.2 select_reduce_fusion
  22.6 0.1 reduce_sum.31
  22.8 0.1 copy.25
  22.9 0.7 multiply_add_fusion
  23.6 0.7 convert_element_type.75
  24.2 0.7 convert_element_type.84
  24.9 0.0 collective-permute-done
  24.9 0.0 copy-done
  24.9 2.2 fusion.16
  27.2 3.4 %all-to-all-start = ((bf16[4,64,512]{2,1,0:T(8,128)(2,1)}), bf16[4,64,512]{2,1,0:T(8,128)(2,1)S(1)}, u32[]{:S(2)}, u32[]{:S(2)}) async-start(bf16[4,64,512]{2,1,0:T(8,128)(2,1)} %bitcast.1), calls=%async_computation | async-start | bytes 524288 | tf_op jit(solution)/shard_map/all_to_all | solution.py:56
  30.6 0.0 all-gather.3.cloned.1.call-start
  30.6 5.9 %all-to-all-done = bf16[4,64,512]{2,1,0:T(8,128)(2,1)S(1)} async-done(((bf16[4,64,512]{2,1,0:T(8,128)(2,1)}), bf16[4,64,512]{2,1,0:T(8,128)(2,1)S(1)}, u32[]{:S(2)}, u32[]{:S(2)}) %all-to-all-start) | async-done | bytes 262176 | tf_op jit(solution)/shard_map/all_to_all | solution.py:56
  36.7 0.2 fusion.18
  36.8 0.5 convolution_convert_fusion
  37.3 30.3 %all_to_all.23 = bf16[8,32,2048]{2,1,0:T(8,128)(2,1)} all-to-all(bf16[8,32,2048]{2,1,0:T(8,128)(2,1)S(1)} %bitcast.55), channel_id=1, replica_groups=mesh['sp'=8,'tp'=4] {'sp'}, dimensions={0} | all-to-all | bytes 2097152 | tf_op jit(solution)/shard_map/all_to_all | solution.py:82
  67.6 0.0 all-gather.3.cloned.1.call-update
  67.7 0.0 all-reduce.3.cloned.1.call-start
  67.7 32.8 %all-gather.3.cloned.1.call-done = bf16[8,128,2048]{2,1,0:T(8,128)(2,1)} async-done(((bf16[8,32,2048]{2,1,0:T(8,128)(2,1)}), bf16[8,128,2048]{2,1,0:T(8,128)(2,1)}) %all-gather.3.cloned.1.call-update) | async-done | bytes 4194320 | tf_op jit(solution)/shard_map/all_gather | solution.py:81
  100.5 0.0 copy-start.2
  100.5 0.0 slice-start
  100.5 11.8 %fusion.4 = f32[1024,1792]{1,0:T(8,128)S(1)} fusion(bf16[1024,2048]{1,0:T(8,128)(2,1)} %bitcast.58, bf16[1,2048,1792]{2,1,0:T(8,128)(2,1)} %param.17), kind=kOutput, calls=%fused_computation.4 | convolution fusion | flops 7516192768 | bytes 18874368 | tf_op jit(solution)/shard_map/dot_general | solution.py:18
  112.3 0.0 copy-done.2
  112.3 0.0 slice-start.1
  112.4 11.4 %multiply_convert_fusion = bf16[1024,1792]{1,0:T(8,128)(2,1)S(1)} fusion(f32[1024,1792]{1,0:T(8,128)S(1)} %fusion.4, bf16[1024,2048]{1,0:T(8,128)(2,1)S(1)} %bitcast.59, bf16[1,2048,1792]{2,1,0:T(8,128)(2,1)} %param.18), kind=kOutput, calls=%fused_computation.6 | convolution fusion | flops 7527202816 | bytes 22544384 | tf_op jit(solution)/shard_map/dot_general | solution.py:19
  123.8 0.0 slice-done
  123.8 0.0 slice-done.1
  123.8 0.0 copy-start.3
  123.8 9.3 %fusion.8 = bf16[8,4,32,2048]{3,2,1,0:T(8,128)(2,1)} fusion(bf16[8,4,32,1792]{3,2,1,0:T(8,128)(2,1)S(1)} %bitcast.60, bf16[1,1792,2048]{2,1,0:T(8,128)(2,1)S(1)} %bitcast.57), kind=kOutput, calls=%fused_computation.7 | convolution fusion | flops 7518289920 | bytes 15204352 | tf_op jit(solution)/shard_map/dot_general | solution.py:21
  133.1 0.0 all-reduce.3.cloned.1.call-update
  133.1 0.0 copy-done.3
  133.1 0.6 dynamic-slice
  133.7 85.1 %all-reduce.3.cloned.1.call-done = bf16[8,4,32,2048]{3,2,1,0:T(8,128)(2,1)} async-done(((bf16[8,4,32,2048]{3,2,1,0:T(8,128)(2,1)}), bf16[8,4,32,2048]{3,2,1,0:T(8,128)(2,1)}) %all-reduce.3.cloned.1.call-update) | async-done | bytes 4194320
  218.8 3.0 %dynamic-slice_bitcast_fusion = bf16[8,32,2048]{2,1,0:T(8,128)(2,1)} fusion(bf16[8,4,32,2048]{3,2,1,0:T(8,128)(2,1)} %all-reduce.3.cloned.1.call-done, u32[]{:T(128)} %bitcast.25), kind=kLoop, calls=%fused_computation.20 | loop fusion | bytes 2097156 | tf_op jit(solution)/shard_map/reshape | solution.py:24
  221.7 5.5 %all-to-all-start.2 = ((bf16[8,32,2048]{2,1,0:T(8,128)(2,1)}), bf16[8,32,2048]{2,1,0:T(8,128)(2,1)S(1)}, u32[]{:S(2)}, u32[]{:S(2)}) async-start(bf16[8,32,2048]{2,1,0:T(8,128)(2,1)} %dynamic-slice_bitcast_fusion), calls=%async_computation.2 | async-start | bytes 2097152 | tf_op jit(solution)/shard_map/all_to_all | solution.py:88
  227.2 0.0 copy-done.1
  227.3 25.6 %all-to-all-done.2 = bf16[8,32,2048]{2,1,0:T(8,128)(2,1)S(1)} async-done(((bf16[8,32,2048]{2,1,0:T(8,128)(2,1)}), bf16[8,32,2048]{2,1,0:T(8,128)(2,1)S(1)}, u32[]{:S(2)}, u32[]{:S(2)}) %all-to-all-start.2) | async-done | bytes 1048608 | tf_op jit(solution)/shard_map/all_to_all | solution.py:88
  252.8 0.3 convolution_multiply_fusion
  253.2 1.1 fusion.13
  (11 shorter events, 0.1 us)
Async XLA Ops:
  6.5 18.4 %copy-start = (bf16[1,512,512]{2,1,0:T(8,128)(2,1)S(1)}, bf16[1,512,512]{2,1,0:T(8,128)(2,1)}, u32[]{:S(2)}) copy-start(bf16[1,512,512]{2,1,0:T(8,128)(2,1)} %param.12) | copy-start | bytes 1572868
  17.8 7.1 %collective-permute-start = (bf16[15,512]{1,0:T(8,128)(2,1)S(1)}, bf16[15,512]{1,0:T(8,128)(2,1)S(1)}, u32[]{:S(2)}, u32[]{:S(2)}) collective-permute-start(bf16[15,512]{1,0:T(8,128)(2,1)S(1)} %slice.20), channel_id=1, source_target_pairs={{0,4},{4,8},{8,12},{12,16},{16,20},{20,24},{24,28},{1,5},{5,9},{9,... | collective-permute-start | bytes 46088 | tf_op jit(solution)/shard_map/ppermute | solution.py:12
  27.2 9.4 %all-to-all-start = ((bf16[4,64,512]{2,1,0:T(8,128)(2,1)}), bf16[4,64,512]{2,1,0:T(8,128)(2,1)S(1)}, u32[]{:S(2)}, u32[]{:S(2)}) async-start(bf16[4,64,512]{2,1,0:T(8,128)(2,1)} %bitcast.1), calls=%async_computation | async-start | bytes 524288 | tf_op jit(solution)/shard_map/all_to_all | solution.py:56
  30.6 69.9 %all-gather.3.cloned.1.call-start = ((), (), s32[]{:S(2)}) async-start(), calls=%async_computation.3 | async-start | bytes 5242880 | tf_op jit(solution)/shard_map/all_gather | solution.py:81
  67.7 151.1 %all-reduce.3.cloned.1.call-start = ((), (), s32[]{:S(2)}) async-start(), calls=%async_computation.4 | async-start | bytes 8388608
  100.5 11.8 %copy-start.2 = (bf16[8,128,2048]{2,1,0:T(8,128)(2,1)S(1)}, bf16[8,128,2048]{2,1,0:T(8,128)(2,1)}, u32[]{:S(2)}) copy-start(bf16[8,128,2048]{2,1,0:T(8,128)(2,1)} %all-gather.3.cloned.1.call-done) | copy-start | bytes 12582916
  100.5 23.2 %slice-start = ((s8[7340032]{0:T(1024)(128)(4,1)}), s8[4194304]{0:T(1024)(128)(4,1)S(1)}, s32[]{:S(2)}) async-start(s8[7340032]{0:T(1024)(128)(4,1)} %bitcast.56), calls=%async_computation.5 | async-start | bytes 8388608
  112.3 11.4 %slice-start.1 = ((s8[7340032]{0:T(1024)(128)(4,1)}), s8[3145728]{0:T(1024)(128)(4,1)S(1)}, s32[]{:S(2)}) async-start(s8[7340032]{0:T(1024)(128)(4,1)} %bitcast.56), calls=%async_computation.6 | async-start | bytes 6291456
  123.8 9.3 %copy-start.3 = (u32[32]{0:T(128)S(1)}, u32[32]{0:T(128)}, u32[]{:S(2)}) copy-start(u32[32]{0:T(128)} %constant.46) | copy-start | bytes 388
  133.1 94.2 %copy-start.1 = (f32[64,2]{0,1:T(2,128)S(1)}, f32[64,2]{0,1:T(2,128)}, u32[]{:S(2)}) copy-start(f32[64,2]{0,1:T(2,128)} %param.16) | copy-start | bytes 1540
  221.7 31.1 %all-to-all-start.2 = ((bf16[8,32,2048]{2,1,0:T(8,128)(2,1)}), bf16[8,32,2048]{2,1,0:T(8,128)(2,1)S(1)}, u32[]{:S(2)}, u32[]{:S(2)}) async-start(bf16[8,32,2048]{2,1,0:T(8,128)(2,1)} %dynamic-slice_bitcast_fusion), calls=%async_computation.2 | async-start | bytes 2097152 | tf_op jit(solution)/shard_map/all_to_all | solution.py:88
Sparse Core Ops, SparseCore 0:
  67.8 32.7 all-gather.2
  133.2 85.4 all-reduce.2
where the time goes:
time: 262 us; the launch traced here: 261 us
  waiting for transfers between devices  149 us (57%)
  blocking collectives  38.7 us (15%)
  matrix products  36.6 us (14%)
  between operations  13.6 us (5%)
  starting transfers between devices  12.4 us (5%)
  other arithmetic  5.63 us (2%)
  local copies, waits for them, and re-layouts  4.75 us (2%)
    unnamed x3, waiting for transfers between devices  85.1 us
    all_gather x1, waiting for transfers between devices, per_device(): lax.all_gather(lax.all_to_all(send_rows, 'sp', split_axis=0, concat_axis=...  32.8 us
    all_to_all x1, blocking collectives, per_device(): lax.all_to_all(send_rows, 'sp', split_axis=0, concat_axis=0, tiled=True)  30.3 us
    all_to_all x1, waiting for transfers between devices, per_device(): lax.all_to_all(served, 'sp', split_axis=0, concat_axis=0, tiled=True)  25.6 us
    dot_general x1, matrix products, expert_rows(): gate_val = jnp.dot(flat_rows, w_gate[0], preferred_element_type=jnp.float32)  11.8 us
    dot_general x1, matrix products, expert_rows(): up_val = jnp.dot(flat_rows, w_up[0], preferred_element_type=jnp.float32)  11.4 us
    dot_general x1, matrix products, expert_rows(): block_out = jnp.dot(hidden, w_down[0], preferred_element_type=jnp.float32)  9.28 us
    psum x1, blocking collectives, per_device(): square = lax.psum(jnp.sum(stream_f32 * stream_f32, axis=1), 'tp')  8.37 us
  transfers between devices with their start and end apart: 5, of which 4 were waited for; matrix products, arithmetic and copies ran while one was open for 2% of the time, Pallas kernels for 0%

commit v1 on v0

--- a/solution.py
+++ b/solution.py
@@ -1,6 +1,10 @@
+import functools
+
 import jax
 import jax.numpy as jnp
 from jax import lax
+from jax.experimental import pallas as pl
+from jax.experimental.pallas import tpu as pltpu
 from jax.sharding import PartitionSpec as P
 
 NORM_EPS = 1e-06
@@ -12,16 +16,338 @@
     return lax.ppermute(block, axis, route)
 
 
-def expert_rows(arrived, w_gate, w_up, w_down):
-    sp_count, tp_count, slot_count, model_width = arrived.shape
-    flat_rows = arrived.reshape(-1, model_width)
-    gate_val = jnp.dot(flat_rows, w_gate[0], preferred_element_type=jnp.float32)
-    up_val = jnp.dot(flat_rows, w_up[0], preferred_element_type=jnp.float32)
-    hidden = (jax.nn.silu(gate_val) * up_val).astype(jnp.bfloat16)
-    block_out = jnp.dot(hidden, w_down[0], preferred_element_type=jnp.float32)
-    block_out = block_out.reshape(sp_count, tp_count, slot_count, model_width)
-    summed = lax.psum_scatter(block_out.astype(jnp.bfloat16), "tp", scatter_dimension=1, tiled=True)
-    return summed.reshape(sp_count, slot_count, model_width)
+MESH = pl.DeviceIdType.MESH
+COL_TILE = 256
+LANES = 2
+
+
+def as_rows(block):
+    width = block.shape[-1]
+    if block.shape[-2] % 16:
+        return block.astype(jnp.float32).reshape(-1, width).astype(block.dtype)
+    return block.reshape(-1, width)
+
+
+def col_tile(width):
+    return COL_TILE if width % COL_TILE == 0 else width
+
+
+def expert_kernel(
+    sp_count,
+    tp_count,
+    chunks,
+    send_ref,
+    pick_ref,
+    weight_ref,
+    after_ref,
+    gate_hbm,
+    up_hbm,
+    down_hbm,
+    out_ref,
+    gate,
+    up,
+    down,
+    arrived,
+    hidden,
+    partial,
+    pair_in,
+    pair_sum,
+    side_in,
+    served,
+    returned,
+    local_sem,
+    first_send,
+    first_recv,
+    side_send,
+    side_recv,
+    pair_send,
+    pair_recv,
+    back_pair,
+    back_side,
+    back_send,
+    back_recv,
+):
+    me = lax.axis_index("sp")
+    tp_me = lax.axis_index("tp")
+    high, low = tp_me // LANES, lax.rem(tp_me, LANES)
+    highs = tp_count // LANES
+    other_low = 1 - low
+    pair_id = {"sp": me, "tp": high * LANES + other_low}
+    steps = sp_count // chunks
+    cap, width = send_ref.shape[1:]
+    ff_width = gate.shape[1]
+
+    def side_high(distance):
+        return lax.rem(high + distance, highs)
+
+    def side_id(distance):
+        return {"sp": me, "tp": side_high(distance) * LANES + low}
+
+    def from_high(distance):
+        return lax.rem(high - distance + highs, highs)
+
+    weight_copies = [
+        pltpu.make_async_copy(source.at[0], target, local_sem.at[index])
+        for index, (source, target) in enumerate(((gate_hbm, gate), (up_hbm, up), (down_hbm, down)))
+    ]
+    own_copy = pltpu.make_async_copy(send_ref.at[0], arrived.at[0, low, high], local_sem.at[3])
+    own_copy.start()
+
+    barrier = pltpu.get_barrier_semaphore()
+    for step in range(1, sp_count):
+        pl.semaphore_signal(
+            barrier,
+            inc=1,
+            device_id={"sp": lax.rem(me + step, sp_count), "tp": tp_me},
+            device_id_type=MESH,
+        )
+    for distance in range(1, highs):
+        pl.semaphore_signal(barrier, inc=1, device_id=side_id(distance), device_id_type=MESH)
+    pl.semaphore_signal(barrier, inc=1, device_id=pair_id, device_id_type=MESH)
+    pl.semaphore_wait(barrier, sp_count - 1 + highs - 1 + 1)
+
+    def first_copy(step):
+        return pltpu.make_async_remote_copy(
+            src_ref=send_ref.at[step],
+            dst_ref=arrived.at[step, low, high],
+            send_sem=first_send.at[step],
+            recv_sem=first_recv.at[step],
+            device_id={"sp": lax.rem(me + step, sp_count), "tp": tp_me},
+            device_id_type=MESH,
+        )
+
+    def side_copy(step, distance):
+        return pltpu.make_async_remote_copy(
+            src_ref=arrived.at[step, low, high],
+            dst_ref=arrived.at[step, low, high],
+            send_sem=side_send.at[step, distance - 1],
+            recv_sem=side_recv.at[step, distance - 1],
+            device_id=side_id(distance),
+            device_id_type=MESH,
+        )
+
+    def pair_copy(step, distance):
+        block = arrived.at[step, low, from_high(distance)]
+        return pltpu.make_async_remote_copy(
+            src_ref=block,
+            dst_ref=block,
+            send_sem=pair_send.at[step, distance],
+            recv_sem=pair_recv.at[step, distance],
+            device_id=pair_id,
+            device_id_type=MESH,
+        )
+
+    def chunk_steps(chunk):
+        return range(chunk * steps, (chunk + 1) * steps)
+
+    def spread(chunk):
+        for step in chunk_steps(chunk):
+            if step == 0:
+                own_copy.wait()
+            else:
+                first_copy(step).wait_recv()
+            for distance in range(1, highs):
+                side_copy(step, distance).start()
+            pair_copy(step, 0).start()
+
+    def pass_on(chunk):
+        for step in chunk_steps(chunk):
+            for distance in range(1, highs):
+                side_copy(step, distance).wait_recv()
+                pair_copy(step, distance).start()
+
+    def settle(chunk):
+        for step in chunk_steps(chunk):
+            for distance in range(highs):
+                pair_copy(step, distance).wait_recv()
+
+    def span(chunk):
+        return pl.ds(chunk * steps, steps)
+
+    def gate_up(chunk):
+        tile = col_tile(ff_width)
+
+        def body(index, carry):
+            columns = pl.ds(pl.multiple_of(index * tile, tile), tile)
+            rows = as_rows(arrived[span(chunk)])
+            gate_val = jnp.dot(rows, gate[:, columns], preferred_element_type=jnp.float32)
+            up_val = jnp.dot(rows, up[:, columns], preferred_element_type=jnp.float32)
+            hidden[:, columns] = (jax.nn.silu(gate_val) * up_val).astype(jnp.bfloat16)
+            return carry
+
+        lax.fori_loop(0, ff_width // tile, body, 0)
+
+    def project(chunk):
+        tile = col_tile(width)
+
+        def body(index, carry):
+            columns = pl.ds(pl.multiple_of(index * tile, tile), tile)
+            block = jnp.dot(hidden[...], down[:, columns], preferred_element_type=jnp.float32)
+            block = block.reshape(steps, LANES, highs, cap, tile).astype(jnp.bfloat16)
+            partial[span(chunk), :, :, :, columns] = block
+            return carry
+
+        lax.fori_loop(0, width // tile, body, 0)
+
+    def back_pair_copy(chunk):
+        return pltpu.make_async_remote_copy(
+            src_ref=partial.at[span(chunk), other_low],
+            dst_ref=pair_in.at[span(chunk)],
+            send_sem=back_pair.at[0, chunk],
+            recv_sem=back_pair.at[1, chunk],
+            device_id=pair_id,
+            device_id_type=MESH,
+        )
+
+    def back_side_copy(chunk, distance):
+        return pltpu.make_async_remote_copy(
+            src_ref=pair_sum.at[distance - 1, span(chunk)],
+            dst_ref=side_in.at[distance - 1, span(chunk)],
+            send_sem=back_side.at[0, chunk, distance - 1],
+            recv_sem=back_side.at[1, chunk, distance - 1],
+            device_id=side_id(distance),
+            device_id_type=MESH,
+        )
+
+    def back_copy(step):
+        return pltpu.make_async_remote_copy(
+            src_ref=served.at[step],
+            dst_ref=returned.at[step],
+            send_sem=back_send.at[step],
+            recv_sem=back_recv.at[step],
+            device_id={"sp": lax.rem(me - step + sp_count, sp_count), "tp": tp_me},
+            device_id_type=MESH,
+        )
+
+    def pair_add(chunk):
+        back_pair_copy(chunk).wait_recv()
+        for distance in range(1, highs):
+            target = side_high(distance)
+
+            def body(index, carry, distance=distance, target=target):
+                step = chunk * steps + index
+                total = partial[step, low, target].astype(jnp.float32)
+                total = total + pair_in[step, target].astype(jnp.float32)
+                pair_sum[distance - 1, step] = total.astype(jnp.bfloat16)
+                return carry
+
+            lax.fori_loop(0, steps, body, 0)
+            back_side_copy(chunk, distance).start()
+
+    def side_add(chunk):
+        for distance in range(1, highs):
+            back_side_copy(chunk, distance).wait_recv()
+        for step in chunk_steps(chunk):
+            total = partial[step, low, high].astype(jnp.float32)
+            total = total + pair_in[step, high].astype(jnp.float32)
+            for distance in range(1, highs):
+                total = total + side_in[distance - 1, step].astype(jnp.float32)
+            if step == 0:
+                returned[0] = total.astype(jnp.bfloat16)
+            else:
+                served[step] = total.astype(jnp.bfloat16)
+                back_copy(step).start()
+
+    for step in range(1, sp_count):
+        first_copy(step).start()
+    for copy in weight_copies:
+        copy.start()
+
+    spread(0)
+    for chunk in range(1, chunks - 1):
+        spread(chunk)
+    pass_on(0)
+    settle(0)
+    for copy in weight_copies[:2]:
+        copy.wait()
+    for chunk in range(chunks):
+        gate_up(chunk)
+        if chunk == 0:
+            if chunks > 1:
+                spread(chunks - 1)
+            weight_copies[2].wait()
+        if chunk + 1 < chunks:
+            pass_on(chunk + 1)
+        if chunk >= 1:
+            pair_add(chunk - 1)
+        if chunk >= 2:
+            side_add(chunk - 2)
+        project(chunk)
+        back_pair_copy(chunk).start()
+        if chunk + 1 < chunks:
+            settle(chunk + 1)
+    pair_add(chunks - 1)
+    if chunks > 1:
+        side_add(chunks - 2)
+    side_add(chunks - 1)
+
+    for step in range(1, sp_count):
+        back_copy(step).wait_recv()
+    rows = as_rows(returned[...])
+    total = after_ref[...].astype(jnp.float32)
+    for pick in range(pick_ref.shape[0]):
+        picked = jnp.dot(pick_ref[pick], rows, preferred_element_type=jnp.float32)
+        total = total + weight_ref[:, pick : pick + 1] * picked
+    out_ref[...] = total.astype(jnp.bfloat16)
+
+    for step in range(sp_count):
+        if step > 0:
+            first_copy(step).wait_send()
+            back_copy(step).wait_send()
+        for distance in range(1, highs):
+            side_copy(step, distance).wait_send()
+        for distance in range(highs):
+            pair_copy(step, distance).wait_send()
+    for chunk in range(chunks):
+        back_pair_copy(chunk).wait_send()
+        for distance in range(1, highs):
+            back_side_copy(chunk, distance).wait_send()
+
+
+def routed_experts(send_rows, picks, route_weight, after, w_gate, w_up, w_down):
+    sp_count, cap, width = send_rows.shape
+    tp_count = lax.axis_size("tp")
+    highs = tp_count // LANES
+    chunks = 4 if sp_count % 4 == 0 else 1
+    chunk_rows = sp_count // chunks * tp_count * cap
+    ff_width = w_gate.shape[2]
+    half = jnp.bfloat16
+    vmem = pl.BlockSpec(memory_space=pltpu.VMEM)
+    hbm = pl.BlockSpec(memory_space=pl.ANY)
+    dma = pltpu.SemaphoreType.DMA
+    return pl.pallas_call(
+        functools.partial(expert_kernel, sp_count, tp_count, chunks),
+        out_shape=jax.ShapeDtypeStruct(after.shape, half),
+        in_specs=[vmem] * 4 + [hbm] * 3,
+        out_specs=vmem,
+        scratch_shapes=[
+            pltpu.VMEM(w_gate.shape[1:], half),
+            pltpu.VMEM(w_up.shape[1:], half),
+            pltpu.VMEM(w_down.shape[1:], half),
+            pltpu.VMEM((sp_count, LANES, highs, cap, width), half),
+            pltpu.VMEM((chunk_rows, ff_width), half),
+            pltpu.VMEM((sp_count, LANES, highs, cap, width), half),
+            pltpu.VMEM((sp_count, highs, cap, width), half),
+            pltpu.VMEM((highs - 1, sp_count, cap, width), half),
+            pltpu.VMEM((highs - 1, sp_count, cap, width), half),
+            pltpu.VMEM((sp_count, cap, width), half),
+            pltpu.VMEM((sp_count, cap, width), half),
+            dma((4,)),
+            dma((sp_count,)),
+            dma((sp_count,)),
+            dma((sp_count, highs - 1)),
+            dma((sp_count, highs - 1)),
+            dma((sp_count, highs)),
+            dma((sp_count, highs)),
+            dma((2, chunks)),
+            dma((2, chunks, highs - 1)),
+            dma((sp_count,)),
+            dma((sp_count,)),
+        ],
+        compiler_params=pltpu.CompilerParams(
+            collective_id=1, has_side_effects=True, vmem_limit_bytes=60 * 1024 * 1024
+        ),
+    )(send_rows, picks, route_weight, after, w_gate, w_up, w_down)
 
 
 def per_device(
@@ -65,34 +391,16 @@
     )
     slot_rank = jnp.cumsum(is_expert, axis=0) - is_expert
     slot_index = jnp.sum(slot_rank * is_expert, axis=1)
-    dest_slot = (flat_routes * capacity + slot_index).reshape(tok_count, top_count)
+    step_away = lax.rem(flat_routes - lax.axis_index("sp") + sp_count, sp_count)
+    dest_slot = (step_away * capacity + slot_index).reshape(tok_count, top_count)
     slot_ids = jnp.arange(sp_count * capacity, dtype=jnp.int32)
-    pick_masks = [
-        (dest_slot[:, pick_index][None, :] == slot_ids[:, None]).astype(jnp.bfloat16)
-        for pick_index in range(top_count)
-    ]
-    dispatch_mask = pick_masks[0]
-    pick_index = 1
-    dispatch_mask = dispatch_mask + pick_masks[pick_index]
+    picks = (dest_slot.T[:, :, None] == slot_ids[None, None, :]).astype(jnp.bfloat16)
+    dispatch_mask = jnp.sum(picks, axis=0).T
     send_rows = jnp.dot(dispatch_mask, normed2, preferred_element_type=jnp.float32).astype(
         jnp.bfloat16
     )
     send_rows = send_rows.reshape(sp_count, capacity, model_width)
-    shared = lax.all_gather(
-        lax.all_to_all(send_rows, "sp", split_axis=0, concat_axis=0, tiled=True)[:, None],
-        "tp",
-        axis=1,
-        tiled=True,
-    )
-    served = expert_rows(shared, w_gate, w_up, w_down)
-    returned = lax.all_to_all(served, "sp", split_axis=0, concat_axis=0, tiled=True).reshape(
-        sp_count * capacity, model_width
-    )
-    expert_sum = after_f32
-    for pick_index in range(top_count):
-        picked_out = jnp.dot(pick_masks[pick_index].T, returned, preferred_element_type=jnp.float32)
-        expert_sum = expert_sum + route_weight[:, pick_index : pick_index + 1] * picked_out
-    return expert_sum.astype(jnp.bfloat16)
+    return routed_experts(send_rows, picks, route_weight, token_rows, w_gate, w_up, w_down)
 
 
 def solution(mesh):

time: 262 us -> 122 us (0.47)
  waiting for transfers between devices: 149 us -> 5.28 us
  Pallas kernels: 0 us -> 86.7 us
  matrix products: 36.6 us -> 3.71 us
  blocking collectives: 38.7 us -> 8.37 us
  between operations: 13.6 us -> 0.12 us
  starting transfers between devices: 12.4 us -> 6.83 us
    pallas_call x0 -> x1, Pallas kernels: none -> 86.7 us  [routed_experts(): pl.pallas_call(functools.partial(expert_kernel, sp_count, tp_count, chunk...]
    unnamed x3 -> x0, waiting for transfers between devices: 85.1 us -> none
    dot_general x5 -> x0, matrix products: 33.9 us -> none  [the longest x1 11.8 us: expert_rows(): gate_val = jnp.dot(flat_rows, w_gate[0], preferred_element_type=jnp.float32)]
    all_gather x1 -> x0, waiting for transfers between devices: 32.8 us -> none  [per_device(): lax.all_gather(lax.all_to_all(send_rows, 'sp', split_axis=0, concat_axis=...]
    all_to_all x1 -> x0, blocking collectives: 30.3 us -> none  [per_device(): lax.all_to_all(send_rows, 'sp', split_axis=0, concat_axis=0, tiled=True)]
    all_to_all x1 -> x0, waiting for transfers between devices: 25.6 us -> none  [per_device(): lax.all_to_all(served, 'sp', split_axis=0, concat_axis=0, tiled=True)]
    all_to_all x1 -> x0, starting transfers between devices: 5.52 us -> none  [per_device(): lax.all_to_all(served, 'sp', split_axis=0, concat_axis=0, tiled=True)]
    reshape x1 -> x0, local copies, waits for them, and re-layouts: 2.97 us -> none  [expert_rows(): return summed.reshape(sp_count, slot_count, model_width)]
  transfers between devices with their start and end apart: 5 -> 2, of which waited for: 4 -> 1; matrix products, arithmetic and copies ran while one was open for 2% -> 5% of each run, Pallas kernels for 0% -> 0%
where the time goes in v1:
time: 122 us
  Pallas kernels  86.7 us (71%)
  blocking collectives  8.37 us (7%)
  starting transfers between devices  6.83 us (6%)
  other arithmetic  6.37 us (5%)
  waiting for transfers between devices  5.28 us (4%)
  local copies, waits for them, and re-layouts  4.2 us (3%)
  matrix products  3.71 us (3%)
    pallas_call x1, Pallas kernels, routed_experts(): pl.pallas_call(functools.partial(expert_kernel, sp_count, tp_count, chunk...  86.7 us
    psum x1, blocking collectives, per_device(): square = lax.psum(jnp.sum(stream_f32 * stream_f32, axis=1), 'tp')  8.37 us
    all_to_all x1, waiting for transfers between devices, per_device(): lax.all_to_all(after_mix, 'tp', split_axis=0, concat_axis=1, tiled=True)  5.27 us
    unnamed x7, local copies, waits for them, and re-layouts  3.82 us
    ppermute x1, starting transfers between devices, passed_along(): return lax.ppermute(block, axis, route)  3.42 us
    all_to_all x1, starting transfers between devices, per_device(): lax.all_to_all(after_mix, 'tp', split_axis=0, concat_axis=1, tiled=True)  3.41 us
  transfers between devices with their start and end apart: 2, of which 1 were waited for; matrix products, arithmetic and copies ran while one was open for 5% of the time, Pallas kernels for 0%

profile of v1, /device:TPU:0, one launch (start us, length us, event | category | flops | bytes accessed | tf_op | source)
XLA Modules:
  0.0 121.6 jit_solution(322282027440570324)
XLA Ops:
  0.0 0.0 copy-start
  0.0 1.1 fusion.4
  1.1 8.4 %psum.7 = f32[256]{0:T(256)S(1)} all-reduce(f32[256]{0:T(256)S(1)} %fusion.4), channel_id=1, replica_groups=mesh['sp'=8,'tp'=4] {'tp'}, use_global_device_ids=true, to_apply=%region_4.5 | all-reduce | flops 256 | bytes 2048 | tf_op jit(solution)/shard_map/psum | solution.py:361
  9.5 0.7 convert_element_type.55
  10.2 1.1 fusion.6
  11.3 3.4 %collective-permute-start = (bf16[15,512]{1,0:T(8,128)(2,1)S(1)}, bf16[15,512]{1,0:T(8,128)(2,1)S(1)}, u32[]{:S(2)}, u32[]{:S(2)}) collective-permute-start(bf16[15,512]{1,0:T(8,128)(2,1)S(1)} %slice.4), channel_id=1, source_target_pairs={{0,4},{4,8},{8,12},{12,16},{16,20},{20,24},{24,28},{1,5},{5,9},{9,... | collective-permute-start | bytes 46088 | tf_op jit(solution)/shard_map/ppermute | solution.py:16
  14.8 0.8 copy.44
  15.5 0.1 eq.28
  15.7 0.1 fusion.30
  15.8 0.2 reduce_window_sum.11
  15.9 0.2 select_reduce_fusion
  16.1 0.1 reduce_sum.42
  16.3 0.1 copy.45
  16.3 0.7 fusion.35
  17.0 0.1 fusion.31
  17.1 0.7 convert_element_type.60
  17.8 0.7 convert_element_type.64
  18.5 1.4 %copy.47.weight_ref = f32[64,2]{1,0:T(8,128)} copy(f32[64,2]{0,1:T(2,128)} %param.16) | data formatting | bytes 1024 | tf_op args[6]
  19.9 0.0 collective-permute-done
  19.9 0.0 copy-done
  19.9 2.2 %fusion.2 = bf16[256,512]{1,0:T(8,128)(2,1)} fusion(bf16[256,512]{1,0:T(8,128)(2,1)} %param.10, bf16[1,512,512]{2,1,0:T(8,128)(2,1)S(1)} %copy-done, bf16[256,512]{1,0:T(8,128)(2,1)S(1)} %fusion.6, bf16[15,512]{1,0:T(8,128)(2,1)S(1)} %collective-permute-done, f32[512]{0:T(512)S(1)} %convert_element_type.60, f32[256]{0:T(256)S(1)} %get-tuple-element.5, ...), kind=kOutput, calls=%fused_computation.5 | convolution fusion | flops 207139840 | bytes 1331264 | tf_op jit(solution)/shard_map/dot_general | solution.py:379
  22.1 3.4 %all-to-all-start = ((bf16[4,64,512]{2,1,0:T(8,128)(2,1)}), bf16[4,64,512]{2,1,0:T(8,128)(2,1)S(1)}, u32[]{:S(2)}, u32[]{:S(2)}) async-start(bf16[4,64,512]{2,1,0:T(8,128)(2,1)} %bitcast.2), calls=%async_computation | async-start | bytes 524288 | tf_op jit(solution)/shard_map/all_to_all | solution.py:382
  25.5 0.7 fusion.29.pick_ref
  26.2 5.3 %all-to-all-done = bf16[4,64,512]{2,1,0:T(8,128)(2,1)S(1)} async-done(((bf16[4,64,512]{2,1,0:T(8,128)(2,1)}), bf16[4,64,512]{2,1,0:T(8,128)(2,1)S(1)}, u32[]{:S(2)}, u32[]{:S(2)}) %all-to-all-start) | async-done | bytes 262176 | tf_op jit(solution)/shard_map/all_to_all | solution.py:382
  31.5 0.2 multiply_reduce_fusion
  31.7 0.0 copy-start.1
  31.7 1.5 %convolution_convert_fusion = bf16[256,2048]{1,0:T(8,128)(2,1)} fusion(bf16[64,256]{1,0:T(8,128)(2,1)S(1)} %fusion.31, bf16[64,2048]{1,0:T(8,128)(2,1)S(1)} %bitcast.13, f32[2048]{0:T(1024)S(1)} %convert_element_type.64, f32[64]{0:T(128)S(1)} %add_rsqrt_fusion.1), kind=kOutput, calls=%fused_computation | convolution fusion | flops 68157440 | bytes 1351936 | tf_op jit(solution)/shard_map/dot_general | solution.py:399
  33.2 0.0 copy-done.1
  33.2 86.7 %shard_map.100 = bf16[64,2048]{1,0:T(8,128)(2,1)} custom-call(bf16[8,32,2048]{2,1,0:T(8,128)(2,1)} %bitcast.12, bf16[2,64,256]{2,1,0:T(8,128)(2,1)} %fusion.29.pick_ref, f32[64,2]{1,0:T(8,128)} %copy.47.weight_ref, bf16[64,2048]{1,0:T(8,128)(2,1)} %bitcast.14, bf16[1,2048,1792]{2,1,0:T(8,128)(2,1)} %gate_hbm.1, bf16[1,2048,1792]{2,1,0:T(8,128)(2,1)} %up_hbm.1, ...), custom_call_target="tpu_custom_call" | custom-call | tf_op jit(solution)/shard_map/pallas_call | solution.py:318
  119.9 1.7 %copy.50 = bf16[64,2048]{1,0:T(8,128)(2,1)} copy(bf16[64,2048]{1,0:T(8,128)(2,1)} %shard_map.100) | data formatting | bytes 524288
  (6 shorter events, 0.1 us)
Async XLA Ops:
  0.0 19.9 %copy-start = (bf16[1,512,512]{2,1,0:T(8,128)(2,1)S(1)}, bf16[1,512,512]{2,1,0:T(8,128)(2,1)}, u32[]{:S(2)}) copy-start(bf16[1,512,512]{2,1,0:T(8,128)(2,1)} %param.12) | copy-start | bytes 1572868
  11.3 8.6 %collective-permute-start = (bf16[15,512]{1,0:T(8,128)(2,1)S(1)}, bf16[15,512]{1,0:T(8,128)(2,1)S(1)}, u32[]{:S(2)}, u32[]{:S(2)}) collective-permute-start(bf16[15,512]{1,0:T(8,128)(2,1)S(1)} %slice.4), channel_id=1, source_target_pairs={{0,4},{4,8},{8,12},{12,16},{16,20},{20,24},{24,28},{1,5},{5,9},{9,... | collective-permute-start | bytes 46088 | tf_op jit(solution)/shard_map/ppermute | solution.py:16
  22.1 9.4 %all-to-all-start = ((bf16[4,64,512]{2,1,0:T(8,128)(2,1)}), bf16[4,64,512]{2,1,0:T(8,128)(2,1)S(1)}, u32[]{:S(2)}, u32[]{:S(2)}) async-start(bf16[4,64,512]{2,1,0:T(8,128)(2,1)} %bitcast.2), calls=%async_computation | async-start | bytes 524288 | tf_op jit(solution)/shard_map/all_to_all | solution.py:382
  31.7 1.5 %copy-start.1 = (bf16[4,8,8,512]{3,2,0,1:T(8,128)(2,1)}, bf16[4,8,8,512]{3,2,0,1:T(8,128)(2,1)S(1)}, u32[]{:S(2)}) copy-start(bf16[4,8,8,512]{3,2,0,1:T(8,128)(2,1)S(1)} %copy.48) | copy-start | bytes 786436

commit v2 on v1

v2 whole, which is shorter than its diff:
```python
import functools

import jax
import jax.numpy as jnp
from jax import lax
from jax.experimental import pallas as pl
from jax.experimental.pallas import tpu as pltpu
from jax.sharding import PartitionSpec as P

NORM_EPS = 1e-06


MESH = pl.DeviceIdType.MESH
COL_TILE = 256
LANES = 2


def as_rows(block):
    width = block.shape[-1]
    if block.shape[-2] % 16:
        return block.astype(jnp.float32).reshape(-1, width).astype(block.dtype)
    return block.reshape(-1, width)


def moves(sp_count):
    far = [(pairs, inner) for pairs in range(1, sp_count // LANES) for inner in range(LANES)]
    return [(0, 0)] + far + [(0, 1)]


def slot_of(expert, me, sp_count):
    pairs = (expert >> 1) - me // LANES
    pairs = jnp.where(pairs < 0, pairs + sp_count // LANES, pairs)
    inner = jnp.where((expert & 1) == lax.rem(me, LANES), 0, 1)
    return jnp.where(pairs == 0, inner * (sp_count - 1), pairs * LANES - 1 + inner)


def as_column(row):
    size = row.shape[1]
    rows = lax.broadcasted_iota(jnp.int32, (size, size), 0)
    columns = lax.broadcasted_iota(jnp.int32, (size, size), 1)
    return jnp.sum(jnp.where(rows == columns, row, 0.0), axis=1, keepdims=True)


def as_row(column):
    size = column.shape[0]
    rows = lax.broadcasted_iota(jnp.int32, (size, size), 0)
    columns = lax.broadcasted_iota(jnp.int32, (size, size), 1)
    return jnp.sum(jnp.where(rows == columns, column, 0.0), axis=0, keepdims=True)


def moved(me, move, sp_count):
    pairs_count = sp_count // LANES
    pairs = lax.rem(me // LANES + move[0], pairs_count)
    return pairs * LANES + lax.rem(me + move[1], LANES)


def moved_back(me, move, sp_count):
    pairs_count = sp_count // LANES
    pairs = lax.rem(me // LANES - move[0] + pairs_count, pairs_count)
    return pairs * LANES + lax.rem(me + move[1], LANES)


def chunk_sizes(sp_count):
    if sp_count % 8:
        return [sp_count]
    return [unit * (sp_count // 8) for unit in (1, 2, 2, 2, 1)]


def col_tile(width):
    return COL_TILE if width % COL_TILE == 0 else width


def expert_kernel(
    sp_count,
    tp_count,
    cap,
    stream_ref,
    mix_ref,
    pool_ref,
    scale_ref,
    gain_ref,
    routes_ref,
    weight_ref,
    gate_hbm,
    up_hbm,
    down_hbm,
    out_ref,
    squares,
    tail,
    halo,
    mixed,
    tokens,
    picked_at,
    send_ref,
    gate,
    up,
    down,
    arrived,
    hidden,
    partial,
    pair_in,
    pair_sum,
    side_in,
    served,
    returned,
    square_sem,
    halo_sem,
    token_sem,
    local_sem,
    first_send,
    first_recv,
    side_send,
    side_recv,
    pair_send,
    pair_recv,
    back_pair,
    back_side,
    back_send,
    back_recv,
):
    me = lax.axis_index("sp")
    tp_me = lax.axis_index("tp")
    high, low = tp_me // LANES, lax.rem(tp_me, LANES)
    highs = tp_count // LANES
    other_low = 1 - low
    pair_id = {"sp": me, "tp": high * LANES + other_low}
    route = moves(sp_count)
    sizes = chunk_sizes(sp_count)
    chunks = len(sizes)
    starts = [sum(sizes[:index]) for index in range(chunks)]
    width = send_ref.shape[2]
    ff_width = gate.shape[1]
    half_width = width // 2

    def side_high(distance):
        return lax.rem(high + distance, highs)

    def side_id(distance):
        return {"sp": me, "tp": side_high(distance) * LANES + low}

    def from_high(distance):
        return lax.rem(high - distance + highs, highs)

    def tp_id(distance):
        return {"sp": me, "tp": lax.rem(tp_me + distance, tp_count)}

    def from_tp(distance):
        return lax.rem(tp_me - distance + tp_count, tp_count)

    weight_copies = [
        pltpu.make_async_copy(source.at[0], target, local_sem.at[index])
        for index, (source, target) in enumerate(((gate_hbm, gate), (up_hbm, up), (down_hbm, down)))
    ]
    own_copy = pltpu.make_async_copy(send_ref.at[0], arrived.at[0, low, high], local_sem.at[3])
    for copy in weight_copies:
        copy.start()

    barrier = pltpu.get_barrier_semaphore()
    for step in range(1, sp_count):
        pl.semaphore_signal(
            barrier,
            inc=1,
            device_id={"sp": moved(me, route[step], sp_count), "tp": tp_me},
            device_id_type=MESH,
        )
    for distance in range(1, tp_count):
        pl.semaphore_signal(barrier, inc=1, device_id=tp_id(distance), device_id_type=MESH)

    def square_copy(distance):
        return pltpu.make_async_remote_copy(
            src_ref=squares.at[0],
            dst_ref=squares.at[distance],
            send_sem=square_sem.at[0, distance - 1],
            recv_sem=square_sem.at[1, distance - 1],
            device_id=tp_id(distance),
            device_id_type=MESH,
        )

    halo_copy = pltpu.make_async_remote_copy(
        src_ref=tail,
        dst_ref=halo,
        send_sem=halo_sem.at[0],
        recv_sem=halo_sem.at[1],
        device_id={"sp": lax.rem(me + 1, sp_count), "tp": tp_me},
        device_id_type=MESH,
    )

    def token_copy(distance):
        return pltpu.make_async_remote_copy(
            src_ref=mixed.at[lax.rem(tp_me + distance, tp_count)],
            dst_ref=tokens.at[tp_me],
            send_sem=token_sem.at[0, distance - 1],
            recv_sem=token_sem.at[1, distance - 1],
            device_id=tp_id(distance),
            device_id_type=MESH,
        )

    tok_rows, group_width = stream_ref.shape
    halo_rows = halo.shape[0]
    tok_count = tokens.shape[1]
    top_count = routes_ref.shape[0]
    slot_count = sp_count * cap
    stream_f32 = stream_ref[...].astype(jnp.float32)
    own_square = as_row(jnp.sum(stream_f32 * stream_f32, axis=1, keepdims=True))
    squares[0] = jnp.broadcast_to(own_square, squares.shape[1:])
    pl.semaphore_wait(barrier, sp_count - 1 + tp_count - 1)
    for distance in range(1, tp_count):
        square_copy(distance).start()

    experts = lax.broadcasted_iota(jnp.int32, (128, tok_count), 0)
    named = [experts == routes_ref[pick : pick + 1, :] for pick in range(top_count)]
    hits = named[0].astype(jnp.float32)
    for pick in range(1, top_count):
        hits = hits + named[pick].astype(jnp.float32)
    earlier = lax.broadcasted_iota(jnp.int32, (tok_count, tok_count), 0)
    later = lax.broadcasted_iota(jnp.int32, (tok_count, tok_count), 1)
    before = jnp.where(earlier < later, 1.0, 0.0).astype(jnp.bfloat16)
    rank = jnp.dot(hits.astype(jnp.bfloat16), before, preferred_element_type=jnp.float32)
    slots = lax.broadcasted_iota(jnp.int32, (slot_count, tok_count), 0).astype(jnp.float32)
    picks = []
    for pick in range(top_count):
        start = slot_of(routes_ref[pick : pick + 1, :], me, sp_count) * cap
        spot = jnp.sum(jnp.where(named[pick], rank, 0.0), axis=0, keepdims=True)
        spot = spot + start.astype(jnp.float32)
        picks.append(jnp.where(slots == spot, 1.0, 0.0))
    dispatch = sum(picks[1:], picks[0]).astype(jnp.bfloat16)
    for pick in range(top_count):
        picked_at[pick] = picks[pick].astype(jnp.bfloat16)

    window_len = jnp.left_shift(jnp.int32(2), tp_me)
    first_row = me * tok_rows
    row_at = lax.broadcasted_iota(jnp.int32, (tok_rows, tok_rows), 0)
    source_at = lax.broadcasted_iota(jnp.int32, (tok_rows, tok_rows), 1)
    lag = row_at - source_at
    band = jnp.where((lag >= 0) & (lag < window_len), 1.0, 0.0).astype(jnp.bfloat16)
    row_at = lax.broadcasted_iota(jnp.int32, (tok_rows, halo_rows), 0)
    source_at = lax.broadcasted_iota(jnp.int32, (tok_rows, halo_rows), 1) - halo_rows
    reach = (row_at - source_at < window_len) & (first_row + source_at >= 0)
    halo_band = jnp.where(reach, 1.0, 0.0).astype(jnp.bfloat16)
    position = first_row + lax.broadcasted_iota(jnp.int32, (tok_rows, 1), 0)
    window_count = jnp.minimum(position + 1, window_len).astype(jnp.float32)

    for distance in range(1, tp_count):
        square_copy(distance).wait_recv()
    square = squares[0, 0:1, :]
    for distance in range(1, tp_count):
        square = square + squares[distance, 0:1, :]
    row_scale = lax.rsqrt(as_column(square) / width + NORM_EPS)
    normed = stream_f32 * row_scale * mix_ref[...].astype(jnp.float32)
    normed = normed.astype(jnp.bfloat16)
    tail[...] = normed[tok_rows - halo_rows :]
    halo_copy.start()
    window_sum = jnp.dot(band, normed, preferred_element_type=jnp.float32)
    halo_copy.wait_recv()
    window_sum = window_sum + jnp.dot(halo_band, halo[...], preferred_element_type=jnp.float32)
    pooled = (window_sum / window_count - normed.astype(jnp.float32)).astype(jnp.bfloat16)
    mixer_out = jnp.dot(pooled, pool_ref[0], preferred_element_type=jnp.float32)
    mixer_out = mixer_out * scale_ref[...].astype(jnp.float32)
    after_mix = (stream_f32 + mixer_out).astype(jnp.bfloat16)
    mixed[...] = after_mix.reshape(mixed.shape)
    for distance in range(1, tp_count):
        token_copy(distance).start()
    tokens[tp_me] = mixed[tp_me]
    for distance in range(1, tp_count):
        token_copy(distance).wait_recv()
    mean_square = jnp.zeros((tok_count, 1), jnp.float32)
    for piece in range(tp_count):
        after_f32 = tokens[piece].astype(jnp.float32)
        mean_square = mean_square + jnp.sum(after_f32 * after_f32, axis=1, keepdims=True)
    ffn_scale = lax.rsqrt(mean_square / width + NORM_EPS)
    for piece in range(tp_count):
        columns = slice(piece * group_width, (piece + 1) * group_width)
        gain = gain_ref[:, columns].astype(jnp.float32)
        normed2 = (tokens[piece].astype(jnp.float32) * ffn_scale * gain).astype(jnp.bfloat16)
        rows = jnp.dot(dispatch, normed2, preferred_element_type=jnp.float32)
        rows = rows.reshape(sp_count, cap, group_width).astype(jnp.bfloat16)
        send_ref[:, :, columns] = rows

    def first_copy(step):
        return pltpu.make_async_remote_copy(
            src_ref=send_ref.at[step],
            dst_ref=arrived.at[step, low, high],
            send_sem=first_send.at[step],
            recv_sem=first_recv.at[step],
            device_id={"sp": moved(me, route[step], sp_count), "tp": tp_me},
            device_id_type=MESH,
        )

    def side_copy(step, distance):
        return pltpu.make_async_remote_copy(
            src_ref=arrived.at[step, low, high],
            dst_ref=arrived.at[step, low, high],
            send_sem=side_send.at[step, distance - 1],
            recv_sem=side_recv.at[step, distance - 1],
            device_id=side_id(distance),
            device_id_type=MESH,
        )

    def pair_copy(step, distance):
        block = arrived.at[step, low, from_high(distance)]
        return pltpu.make_async_remote_copy(
            src_ref=block,
            dst_ref=block,
            send_sem=pair_send.at[step, distance],
            recv_sem=pair_recv.at[step, distance],
            device_id=pair_id,
            device_id_type=MESH,
        )

    def chunk_steps(chunk):
        return range(starts[chunk], starts[chunk] + sizes[chunk])

    def spread(chunk):
        for step in chunk_steps(chunk):
            if step == 0:
                own_copy.wait()
            else:
                first_copy(step).wait_recv()
            for distance in range(1, highs):
                side_copy(step, distance).start()
            pair_copy(step, 0).start()

    def pass_on(chunk):
        for step in chunk_steps(chunk):
            for distance in range(1, highs):
                side_copy(step, distance).wait_recv()
                pair_copy(step, distance).start()

    def settle(chunk):
        for step in chunk_steps(chunk):
            for distance in range(highs):
                pair_copy(step, distance).wait_recv()

    def span(chunk):
        return pl.ds(starts[chunk], sizes[chunk])

    def row_span(chunk):
        return pl.ds(0, sizes[chunk] * tp_count * cap)

    def gate_up(chunk, first, last):
        tile = col_tile(ff_width)

        def body(index, carry):
            columns = pl.ds(pl.multiple_of(index * tile, tile), tile)
            rows = as_rows(arrived[span(chunk)])
            gate_val = jnp.dot(rows, gate[:, columns], preferred_element_type=jnp.float32)
            up_val = jnp.dot(rows, up[:, columns], preferred_element_type=jnp.float32)
            hidden[row_span(chunk), columns] = (jax.nn.silu(gate_val) * up_val).astype(jnp.bfloat16)
            return carry

        lax.fori_loop(first, last, body, 0)

    def project(chunk, half):
        tile = col_tile(half_width)
        first = half * half_width // tile

        def body(index, carry):
            columns = pl.ds(pl.multiple_of(index * tile, tile), tile)
            block = jnp.dot(
                hidden[row_span(chunk), :], down[:, columns], preferred_element_type=jnp.float32
            )
            block = block.reshape(sizes[chunk], LANES, highs, cap, tile).astype(jnp.bfloat16)
            partial[span(chunk), :, :, :, columns] = block
            return carry

        lax.fori_loop(first, first + half_width // tile, body, 0)

    def part(half):
        return pl.ds(half * half_width, half_width)

    def back_pair_copy(chunk, half):
        return pltpu.make_async_remote_copy(
            src_ref=partial.at[span(chunk), other_low, :, :, part(half)],
            dst_ref=pair_in.at[span(chunk), :, :, part(half)],
            send_sem=back_pair.at[0, chunk, half],
            recv_sem=back_pair.at[1, chunk, half],
            device_id=pair_id,
            device_id_type=MESH,
        )

    def back_side_copy(chunk, half, distance):
        return pltpu.make_async_remote_copy(
            src_ref=pair_sum.at[distance - 1, span(chunk), :, part(half)],
            dst_ref=side_in.at[distance - 1, span(chunk), :, part(half)],
            send_sem=back_side.at[0, chunk, half, distance - 1],
            recv_sem=back_side.at[1, chunk, half, distance - 1],
            device_id=side_id(distance),
            device_id_type=MESH,
        )

    def back_copy(step, half):
        return pltpu.make_async_remote_copy(
            src_ref=served.at[step, :, part(half)],
            dst_ref=returned.at[step, :, part(half)],
            send_sem=back_send.at[step, half],
            recv_sem=back_recv.at[step, half],
            device_id={"sp": moved_back(me, route[step], sp_count), "tp": tp_me},
            device_id_type=MESH,
        )

    def pair_add(chunk, half):
        back_pair_copy(chunk, half).wait_recv()
        for distance in range(1, highs):
            target = side_high(distance)

            def body(index, carry, distance=distance, target=target):
                step = starts[chunk] + index
                total = partial[step, low, target, :, part(half)].astype(jnp.float32)
                total = total + pair_in[step, target, :, part(half)].astype(jnp.float32)
                pair_sum[distance - 1, step, :, part(half)] = total.astype(jnp.bfloat16)
                return carry

            lax.fori_loop(0, sizes[chunk], body, 0)
            back_side_copy(chunk, half, distance).start()

    def side_add(chunk, half):
        for distance in range(1, highs):
            back_side_copy(chunk, half, distance).wait_recv()
        for step in chunk_steps(chunk):
            total = partial[step, low, high, :, part(half)].astype(jnp.float32)
            total = total + pair_in[step, high, :, part(half)].astype(jnp.float32)
            for distance in range(1, highs):
                total = total + side_in[distance - 1, step, :, part(half)].astype(jnp.float32)
            if step == 0:
                returned[0, :, part(half)] = total.astype(jnp.bfloat16)
            else:
                served[step, :, part(half)] = total.astype(jnp.bfloat16)
                back_copy(step, half).start()

    own_copy.start()
    for step in range(1, sp_count):
        first_copy(step).start()

    last = chunks - 1
    spread(0)
    pass_on(0)
    if chunks > 1:
        spread(last)
    settle(0)
    for copy in weight_copies:
        copy.wait()
    tiles = ff_width // col_tile(ff_width)
    early, late = tiles // 2, tiles - tiles // 4
    for chunk in range(chunks):
        gate_up(chunk, 0, early)
        if chunk == 0 and chunks > 1:
            pass_on(last)
            spread(1)
        if chunk >= 1:
            pair_add(chunk - 1, 0)
            pair_add(chunk - 1, 1)
        gate_up(chunk, early, late)
        if chunk >= 2:
            side_add(chunk - 2, 0)
            side_add(chunk - 2, 1)
        gate_up(chunk, late, tiles)
        if chunk == 1:
            spread(2)
        if chunk == 2:
            pass_on(3)
        for half in range(2):
            project(chunk, half)
            back_pair_copy(chunk, half).start()
        if chunk < 2 and chunks > 1:
            pass_on(chunk + 1)
        if chunk < last:
            settle(chunk + 1)
        if chunk == 1:
            spread(3)
    pair_add(last, 0)
    pair_add(last, 1)
    for half in range(2):
        if chunks > 1:
            side_add(last - 1, half)
    for half in range(2):
        side_add(last, half)

    for step in range(1, sp_count):
        for half in range(2):
            back_copy(step, half).wait_recv()
    rows = as_rows(returned[...])
    route_weights = [as_column(weight_ref[pick : pick + 1, :]) for pick in range(top_count)]
    for piece in range(tp_count):
        columns = slice(piece * group_width, (piece + 1) * group_width)
        total = tokens[piece].astype(jnp.float32)
        for pick in range(top_count):
            picked = lax.dot_general(
                picked_at[pick],
                rows[:, columns],
                (((0,), (0,)), ((), ())),
                preferred_element_type=jnp.float32,
            )
            total = total + route_weights[pick] * picked
        out_ref[:, columns] = total.astype(jnp.bfloat16)

    halo_copy.wait_send()
    for distance in range(1, tp_count):
        square_copy(distance).wait_send()
        token_copy(distance).wait_send()
    for step in range(sp_count):
        if step > 0:
            first_copy(step).wait_send()
            for half in range(2):
                back_copy(step, half).wait_send()
        for distance in range(1, highs):
            side_copy(step, distance).wait_send()
        for distance in range(highs):
            pair_copy(step, distance).wait_send()
    for chunk in range(chunks):
        for half in range(2):
            back_pair_copy(chunk, half).wait_send()
            for distance in range(1, highs):
                back_side_copy(chunk, half, distance).wait_send()


def per_device(
    stream, mix_gain, pool_weight, pool_scale, ffn_gain, routes, route_weight, w_gate, w_up, w_down
):
    tok_rows, group_width = stream.shape
    tp_count = lax.axis_size("tp")
    sp_count = lax.axis_size("sp")
    width = group_width * tp_count
    tok_count, top_count = routes.shape
    cap = 2 * tok_count * top_count // sp_count
    halo_rows = 2 ** (pool_weight.shape[0] * tp_count)
    highs = tp_count // LANES
    chunks = len(chunk_sizes(sp_count))
    chunk_rows = max(chunk_sizes(sp_count)) * tp_count * cap
    ff_width = w_gate.shape[2]
    half = jnp.bfloat16
    vmem = pl.BlockSpec(memory_space=pltpu.VMEM)
    hbm = pl.BlockSpec(memory_space=pl.ANY)
    dma = pltpu.SemaphoreType.DMA
    return pl.pallas_call(
        functools.partial(expert_kernel, sp_count, tp_count, cap),
        out_shape=jax.ShapeDtypeStruct((tok_count, width), half),
        in_specs=[vmem] * 7 + [hbm] * 3,
        out_specs=vmem,
        scratch_shapes=[
            pltpu.VMEM((tp_count, 8, tok_rows), jnp.float32),
            pltpu.VMEM((halo_rows, group_width), half),
            pltpu.VMEM((halo_rows, group_width), half),
            pltpu.VMEM((tp_count, tok_count, group_width), half),
            pltpu.VMEM((tp_count, tok_count, group_width), half),
            pltpu.VMEM((top_count, sp_count * cap, tok_count), half),
            pltpu.VMEM((sp_count, cap, width), half),
            pltpu.VMEM(w_gate.shape[1:], half),
            pltpu.VMEM(w_up.shape[1:], half),
            pltpu.VMEM(w_down.shape[1:], half),
            pltpu.VMEM((sp_count, LANES, highs, cap, width), half),
            pltpu.VMEM((chunk_rows, ff_width), half),
            pltpu.VMEM((sp_count, LANES, highs, cap, width), half),
            pltpu.VMEM((sp_count, highs, cap, width), half),
            pltpu.VMEM((highs - 1, sp_count, cap, width), half),
            pltpu.VMEM((highs - 1, sp_count, cap, width), half),
            pltpu.VMEM((sp_count, cap, width), half),
            pltpu.VMEM((sp_count, cap, width), half),
            dma((2, tp_count - 1)),
            dma((2,)),
            dma((2, tp_count - 1)),
            dma((4,)),
            dma((sp_count,)),
            dma((sp_count,)),
            dma((sp_count, highs - 1)),
            dma((sp_count, highs - 1)),
            dma((sp_count, highs)),
            dma((sp_count, highs)),
            dma((2, chunks, 2)),
            dma((2, chunks, 2, highs - 1)),
            dma((sp_count, 2)),
            dma((sp_count, 2)),
        ],
        compiler_params=pltpu.CompilerParams(
            collective_id=1, has_side_effects=True, vmem_limit_bytes=60 * 1024 * 1024
        ),
    )(
        stream,
        mix_gain[None, :],
        pool_weight,
        pool_scale[None, :],
        ffn_gain[None, :],
        routes.T,
        route_weight.T,
        w_gate,
        w_up,
        w_down,
    )


def solution(mesh):
    in_specs = (
        P("sp", "tp"),
        P("tp"),
        P("tp", None, None),
        P("tp"),
        P(),
        P(("sp", "tp"), None),
        P(("sp", "tp"), None),
        P("sp", None, "tp"),
        P("sp", None, "tp"),
        P("sp", "tp", None),
    )
    out_specs = P(("sp", "tp"), None)
    return jax.shard_map(
        per_device, mesh=mesh, in_specs=in_specs, out_specs=out_specs, check_vma=False
    )
```

time: 122 us -> 104 us (0.85)
  Pallas kernels: 86.7 us -> 98.7 us
  blocking collectives: 8.37 us -> 0 us
  starting transfers between devices: 6.83 us -> 0 us
  other arithmetic: 6.37 us -> 0 us
  waiting for transfers between devices: 5.28 us -> 0 us
  matrix products: 3.71 us -> 0 us
  local copies, waits for them, and re-layouts: 4.2 us -> 5.47 us
    pallas_call x1, Pallas kernels: 86.7 us -> 98.7 us  [per_device(): pl.pallas_call(functools.partial(expert_kernel, sp_count, tp_count, cap),...]
    psum x1 -> x0, blocking collectives: 8.37 us -> none  [per_device(): square = lax.psum(jnp.sum(stream_f32 * stream_f32, axis=1), 'tp')]
    all_to_all x1 -> x0, waiting for transfers between devices: 5.27 us -> none  [per_device(): lax.all_to_all(after_mix, 'tp', split_axis=0, concat_axis=1, tiled=True)]
    convert_element_type x7 -> x0, other arithmetic: 3.93 us -> none  [the longest x1 1.07 us: per_device(): (stream_f32 * row_scale * mix_gain.astype(jnp.float32)).astype(jnp.bfloat16)]
    broadcast_in_dim x0 -> x3, local copies, waits for them, and re-layouts: none -> 3.8 us  [the longest x1 1.29 us: per_device(): ffn_gain[None, :]]
    dot_general x2 -> x0, matrix products: 3.71 us -> none  [the longest x1 2.23 us: per_device(): jnp.dot(pooled, pool_weight[0], preferred_element_type=jnp.float32)]
    ppermute x1 -> x0, starting transfers between devices: 3.42 us -> none  [passed_along(): return lax.ppermute(block, axis, route)]
    all_to_all x1 -> x0, starting transfers between devices: 3.41 us -> none  [per_device(): lax.all_to_all(after_mix, 'tp', split_axis=0, concat_axis=1, tiled=True)]
  transfers between devices with their start and end apart: 2 -> 0, of which waited for: 1 -> 0; matrix products, arithmetic and copies ran while one was open for 5% -> 0% of each run, Pallas kernels for 0% -> 0%
where the time goes in v2:
time: 104 us
  Pallas kernels  98.7 us (95%)
  local copies, waits for them, and re-layouts  5.47 us (5%)
    pallas_call x1, Pallas kernels, per_device(): pl.pallas_call(functools.partial(expert_kernel, sp_count, tp_count, cap),...  98.7 us

profile of v2, /device:TPU:0, one launch (start us, length us, event | category | flops | bytes accessed | tf_op | source)
XLA Modules:
  0.0 104.2 jit_solution(6972675641152663683)
XLA Ops:
  0.0 1.3 %broadcast_in_dim.9.mix_ref = bf16[1,512]{1,0:T(2,128)(2,1)} reshape(bf16[512]{0:T(512)(128)(2,1)} %param.11) | data formatting | bytes 2048 | tf_op jit(solution)/shard_map/broadcast_in_dim | solution.py:578
  1.3 1.3 %broadcast_in_dim.10.scale_ref = bf16[1,512]{1,0:T(2,128)(2,1)} reshape(bf16[512]{0:T(512)(128)(2,1)} %param.13) | data formatting | bytes 2048 | tf_op jit(solution)/shard_map/broadcast_in_dim | solution.py:580
  2.5 1.3 %broadcast_in_dim.11.gain_ref = bf16[1,2048]{1,0:T(2,128)(2,1)} reshape(bf16[2048]{0:T(1024)(128)(2,1)} %param.14) | data formatting | bytes 8192 | tf_op jit(solution)/shard_map/broadcast_in_dim | solution.py:581
  3.8 98.7 %shard_map.100 = bf16[64,2048]{1,0:T(8,128)(2,1)} custom-call(bf16[256,512]{1,0:T(8,128)(2,1)} %stream_ref.1, bf16[1,512]{1,0:T(2,128)(2,1)} %broadcast_in_dim.9.mix_ref, bf16[1,512,512]{2,1,0:T(8,128)(2,1)} %pool_ref.1, bf16[1,512]{1,0:T(2,128)(2,1)} %broadcast_in_dim.10.scale_ref, bf16[1,2048]{1,0:T(2,128)(2,1)} %broadcast_in_dim.11.gain_ref, ...), custom_call_target="tpu_custom_call" | custom-call | tf_op jit(solution)/shard_map/pallas_call | solution.py:534
  102.5 1.7 %copy.12 = bf16[64,2048]{1,0:T(8,128)(2,1)} copy(bf16[64,2048]{1,0:T(8,128)(2,1)} %shard_map.100) | data formatting | bytes 524288

commit v3 on v2

--- a/solution.py
+++ b/solution.py
@@ -13,6 +13,23 @@
 MESH = pl.DeviceIdType.MESH
 COL_TILE = 256
 LANES = 2
+CHUNK_UNITS = (2, 2, 2, 1, 1)
+PLAN = {
+    "pre": "s0 p0 s1 e0",
+    "0l": "p1 s2",
+    "0z": "e1",
+    "1e": "a0 s3",
+    "1l": "p2 s4",
+    "1z": "e2",
+    "2e": "a1 b0",
+    "2l": "p3 p4",
+    "2z": "e3",
+    "3e": "a2 b1",
+    "3z": "e4",
+    "4e": "a3 b2",
+    "post": "a4 b3 b4",
+}
+SINGLE_PLAN = {"pre": "s0 p0 e0", "post": "a0 b0"}
 
 
 def as_rows(block):
@@ -24,14 +41,14 @@
 
 def moves(sp_count):
     far = [(pairs, inner) for pairs in range(1, sp_count // LANES) for inner in range(LANES)]
-    return [(0, 0)] + far + [(0, 1)]
+    return [(0, 0), (0, 1)] + far
 
 
 def slot_of(expert, me, sp_count):
     pairs = (expert >> 1) - me // LANES
     pairs = jnp.where(pairs < 0, pairs + sp_count // LANES, pairs)
     inner = jnp.where((expert & 1) == lax.rem(me, LANES), 0, 1)
-    return jnp.where(pairs == 0, inner * (sp_count - 1), pairs * LANES - 1 + inner)
+    return pairs * LANES + inner
 
 
 def as_column(row):
@@ -63,7 +80,7 @@
 def chunk_sizes(sp_count):
     if sp_count % 8:
         return [sp_count]
-    return [unit * (sp_count // 8) for unit in (1, 2, 2, 2, 1)]
+    return [unit * (sp_count // 8) for unit in CHUNK_UNITS]
 
 
 def col_tile(width):
@@ -246,7 +263,7 @@
     for distance in range(1, tp_count):
         square = square + squares[distance, 0:1, :]
     row_scale = lax.rsqrt(as_column(square) / width + NORM_EPS)
-    normed = stream_f32 * row_scale * mix_ref[...].astype(jnp.float32)
+    normed = stream_f32 * row_scale * mix_ref[...].astype(jnp.float32)[None, :]
     normed = normed.astype(jnp.bfloat16)
     tail[...] = normed[tok_rows - halo_rows :]
     halo_copy.start()
@@ -255,7 +272,7 @@
     window_sum = window_sum + jnp.dot(halo_band, halo[...], preferred_element_type=jnp.float32)
     pooled = (window_sum / window_count - normed.astype(jnp.float32)).astype(jnp.bfloat16)
     mixer_out = jnp.dot(pooled, pool_ref[0], preferred_element_type=jnp.float32)
-    mixer_out = mixer_out * scale_ref[...].astype(jnp.float32)
+    mixer_out = mixer_out * scale_ref[...].astype(jnp.float32)[None, :]
     after_mix = (stream_f32 + mixer_out).astype(jnp.bfloat16)
     mixed[...] = after_mix.reshape(mixed.shape)
     for distance in range(1, tp_count):
@@ -270,7 +287,7 @@
     ffn_scale = lax.rsqrt(mean_square / width + NORM_EPS)
     for piece in range(tp_count):
         columns = slice(piece * group_width, (piece + 1) * group_width)
-        gain = gain_ref[:, columns].astype(jnp.float32)
+        gain = gain_ref[columns].astype(jnp.float32)[None, :]
         normed2 = (tokens[piece].astype(jnp.float32) * ffn_scale * gain).astype(jnp.bfloat16)
         rows = jnp.dot(dispatch, normed2, preferred_element_type=jnp.float32)
         rows = rows.reshape(sp_count, cap, group_width).astype(jnp.bfloat16)
@@ -431,49 +448,37 @@
     for step in range(1, sp_count):
         first_copy(step).start()
 
-    last = chunks - 1
-    spread(0)
-    pass_on(0)
-    if chunks > 1:
-        spread(last)
-    settle(0)
+    plan = PLAN if chunks == len(CHUNK_UNITS) else SINGLE_PLAN
+    acts = {"s": spread, "p": pass_on, "e": settle}
+    adds = {"a": pair_add, "b": side_add}
+
+    def run(place):
+        for name in plan.get(place, "").split():
+            if name[0] in acts:
+                acts[name[0]](int(name[1]))
+            elif len(name) > 2:
+                adds[name[0]](int(name[1]), int(name[2]))
+            else:
+                for half in range(2):
+                    adds[name[0]](int(name[1]), half)
+
+    run("pre")
     for copy in weight_copies:
         copy.wait()
     tiles = ff_width // col_tile(ff_width)
     early, late = tiles // 2, tiles - tiles // 4
     for chunk in range(chunks):
         gate_up(chunk, 0, early)
-        if chunk == 0 and chunks > 1:
-            pass_on(last)
-            spread(1)
-        if chunk >= 1:
-            pair_add(chunk - 1, 0)
-            pair_add(chunk - 1, 1)
+        run(f"{chunk}e")
         gate_up(chunk, early, late)
-        if chunk >= 2:
-            side_add(chunk - 2, 0)
-            side_add(chunk - 2, 1)
+        run(f"{chunk}m")
         gate_up(chunk, late, tiles)
-        if chunk == 1:
-            spread(2)
-        if chunk == 2:
-            pass_on(3)
+        run(f"{chunk}l")
         for half in range(2):
             project(chunk, half)
             back_pair_copy(chunk, half).start()
-        if chunk < 2 and chunks > 1:
-            pass_on(chunk + 1)
-        if chunk < last:
-            settle(chunk + 1)
-        if chunk == 1:
-            spread(3)
-    pair_add(last, 0)
-    pair_add(last, 1)
-    for half in range(2):
-        if chunks > 1:
-            side_add(last - 1, half)
-    for half in range(2):
-        side_add(last, half)
+            run(f"{chunk}h" if half == 0 else f"{chunk}z")
+    run("post")
 
     for step in range(1, sp_count):
         for half in range(2):
@@ -575,10 +580,10 @@
         ),
     )(
         stream,
-        mix_gain[None, :],
+        mix_gain,
         pool_weight,
-        pool_scale[None, :],
-        ffn_gain[None, :],
+        pool_scale,
+        ffn_gain,
         routes.T,
         route_weight.T,
         w_gate,

time: 104 us -> 95.9 us (0.922)
  Pallas kernels: 98.7 us -> 94 us
  local copies, waits for them, and re-layouts: 5.47 us -> 1.67 us
    pallas_call x1, Pallas kernels: 98.7 us -> 94 us  [per_device(): pl.pallas_call(functools.partial(expert_kernel, sp_count, tp_count, cap),...]
    broadcast_in_dim x3 -> x0, local copies, waits for them, and re-layouts: 3.8 us -> none  [the longest x1 1.29 us: per_device(): ffn_gain[None, :]]
where the time goes in v3:
time: 95.9 us; the launch traced here: 95.7 us
  Pallas kernels  94 us (98%)
  local copies, waits for them, and re-layouts  1.67 us (2%)
    pallas_call x1, Pallas kernels, per_device(): pl.pallas_call(functools.partial(expert_kernel, sp_count, tp_count, cap),...  94 us

profile of v3, /device:TPU:0, one launch (start us, length us, event | category | flops | bytes accessed | tf_op | source)
XLA Modules:
  0.0 95.7 jit_solution(14400592148855992235)
XLA Ops:
  0.0 94.0 %shard_map.100 = bf16[64,2048]{1,0:T(8,128)(2,1)} custom-call(bf16[256,512]{1,0:T(8,128)(2,1)} %stream_ref.1, bf16[512]{0:T(512)(128)(2,1)} %mix_ref.1, bf16[1,512,512]{2,1,0:T(8,128)(2,1)} %pool_ref.1, bf16[512]{0:T(512)(128)(2,1)} %scale_ref.1, bf16[2048]{0:T(1024)(128)(2,1)} %gain_ref.1, s32[2,64]{1,0:T(2,128)} %bitcast.2, f32[2,64]{1,0:T(2,128)} %bitcast.3, ...), custom_call_target="tpu_custom_call" | custom-call | tf_op jit(solution)/shard_map/pallas_call | solution.py:539
  94.0 1.7 %copy.12 = bf16[64,2048]{1,0:T(8,128)(2,1)} copy(bf16[64,2048]{1,0:T(8,128)(2,1)} %shard_map.100) | data formatting | bytes 524288
